TPU v7x, 32 devices: a whole 2x2x4 slice. The times are simulated.
32 devices in a mesh: fs: 8 (over z, y), tp: 4 (over x, core).
Axes of the slice: x: 2, y: 2, z: 4, core: 2. Of those that a mesh axis runs over, the one named last changes fastest.
Arguments:
- tokens: bfloat16 [3072, 2048], P('fs', 'tp'), may hold values from -6 to 6
- norm_gain: float32 [2048], P('fs'), may hold values from 0.1 to 1.9
- gate_train: bfloat16 [8, 2048, 5632], P(None, 'fs', 'tp'), may hold values from -0.125 to 0.125
- up_train: bfloat16 [8, 2048, 5632], P(None, 'fs', 'tp'), may hold values from -0.125 to 0.125
- down_train: bfloat16 [8, 2048, 5632], P(None, 'fs', 'tp'), may hold values from -0.078125 to 0.078125
- routes: int32 [3072, 2], P('fs'), may hold values from 0 to 7, all different within a row; in each aligned block of 384 rows (0 to 383, 384 to 767, ...) at most 192 rows name the same one
- route_logits: float32 [3072, 2], P('fs'), may hold values from -6 to 6
Outputs:
- gate_weights: bfloat16 [8, 2048, 5632], P('fs', None, 'tp')
- up_weights: bfloat16 [8, 2048, 5632], P('fs', None, 'tp')
- down_weights: bfloat16 [8, 2048, 5632], P('fs', None, 'tp')
- mixed: bfloat16 [3072, 2048], P('fs', 'tp')
Inputs may be any that keep to these rules, and one draw needn't show every extreme that they name: `routes`: each row names 2 different experts; among the rows of one device no expert is named more than 192 times, and in every draw some device names some expert exactly 192 times.
All inputs are finite; a program needn't handle non-finite values.
Results may differ from a plain program's by a relative error of at most 0.014.
Values may be sent and summed in bfloat16 or wider, within the bound.
A program may use at most 128 MiB of HBM per device.

v0:
```python
import jax
import jax.numpy as jnp
from jax import lax
from jax.sharding import PartitionSpec as P

EXPERTS = 8


epsilon = 1e-06


def slot_plan(routes, copies, capacity):
    flat_routes = routes.reshape(-1)
    experts_all = jnp.arange(EXPERTS, dtype=jnp.int32)
    onehot = (flat_routes[:, None] == experts_all[None, :]).astype(jnp.int32)
    earlier = jnp.cumsum(onehot, axis=0) - onehot
    order_rank = jnp.sum(earlier * onehot, axis=1)
    target = order_rank % copies * EXPERTS + flat_routes
    return target * capacity + order_rank // copies


def shards(tokens, norm_gain, gate_train, up_train, down_train, routes, route_logits):
    fs_count = lax.axis_size("fs")
    copies = fs_count // EXPERTS
    tok_rows = tokens.shape[0]
    capacity = tok_rows // 2 // copies
    slot_total = fs_count * capacity
    gain_rows = norm_gain[None, :, None]
    gate_low = (gate_train.astype(jnp.float32) * gain_rows).astype(jnp.bfloat16)
    up_low = (up_train.astype(jnp.float32) * gain_rows).astype(jnp.bfloat16)

    def spread(matrix):
        return jnp.tile(matrix, (copies, 1, 1))

    gate_out, up_out, down_out = (
        lax.all_to_all(spread(gate_low), "fs", split_axis=0, concat_axis=1, tiled=True),
        lax.all_to_all(spread(up_low), "fs", split_axis=0, concat_axis=1, tiled=True),
        lax.all_to_all(spread(down_train), "fs", split_axis=0, concat_axis=1, tiled=True),
    )
    slot_index = slot_plan(routes, copies, capacity)
    token_of = jnp.arange(slot_index.shape[0], dtype=jnp.int32) // routes.shape[1]
    owner = jnp.full((slot_total,), tok_rows, jnp.int32).at[slot_index].set(token_of)
    padded = jnp.concatenate([tokens, jnp.zeros((1, tokens.shape[1]), tokens.dtype)], axis=0)
    outgoing = padded[owner]
    arrived = lax.all_to_all(outgoing, "fs", split_axis=0, concat_axis=0, tiled=True)
    arrived = lax.all_gather(arrived, "tp", axis=1, tiled=True)
    arrived_float = arrived.astype(jnp.float32)
    inverse = lax.rsqrt(jnp.mean(arrived_float * arrived_float, axis=1, keepdims=True) + epsilon)
    normed = (arrived_float * inverse).astype(jnp.bfloat16)
    gate_val = jnp.dot(normed, gate_out[0], preferred_element_type=jnp.float32)
    up_val = jnp.dot(normed, up_out[0], preferred_element_type=jnp.float32)
    active = (jax.nn.silu(gate_val) * up_val).astype(jnp.bfloat16)
    down_matrix = down_out[0]
    summed = lax.psum_scatter(
        lax.dot_general(
            down_matrix, active, (((1,), (1,)), ((), ())), preferred_element_type=jnp.float32
        ).astype(jnp.bfloat16),
        "tp",
        scatter_dimension=0,
        tiled=True,
    )
    returned = lax.all_to_all(summed, "fs", split_axis=1, concat_axis=1, tiled=True)
    picked = (
        jnp.take(returned, slot_index, axis=1)
        .astype(jnp.float32)
        .reshape(returned.shape[0], tok_rows, 2)
    )
    first = jax.nn.sigmoid(route_logits[:, 0] - route_logits[:, 1])
    second = jax.nn.sigmoid(route_logits[:, 1] - route_logits[:, 0])
    mixed = picked[:, :, 0] * first[None, :] + picked[:, :, 1] * second[None, :]
    return (gate_out, up_out, down_out, mixed.T.astype(jnp.bfloat16))


def solution(mesh):
    placed = (
        P("fs", "tp"),
        P("fs"),
        P(None, "fs", "tp"),
        P(None, "fs", "tp"),
        P(None, "fs", "tp"),
        P("fs", None),
        P("fs", None),
    )
    return jax.shard_map(
        shards,
        mesh=mesh,
        in_specs=placed,
        out_specs=(P("fs", None, "tp"), P("fs", None, "tp"), P("fs", None, "tp"), P("fs", "tp")),
        check_vma=False,
    )
```

profile of v0, /device:TPU:15, one launch (start us, length us, event | category | flops | bytes accessed | tf_op | source)
XLA Modules:
  0.0 609.5 jit_solution(13876856031865215734)
XLA Ops:
  7.2 0.8 copy.21
  8.0 0.1 eq.31
  8.1 0.1 eq.27
  8.3 0.7 broadcast_multiply_fusion
  9.0 1.7 reduce-window.6
  10.7 0.1 slice.30
  10.8 0.1 copy.23
  10.9 0.2 reduce-window.9
  11.1 0.1 copy.24
  11.2 0.1 copy.26
  11.3 0.2 mul.83
  11.5 0.1 fusion.18
  11.6 3.4 scatter_custom_fusion
  15.0 1.0 concatenate.3
  16.0 0.0 copy-start.4
  16.0 5.4 gather_fusion
  21.4 5.7 all-to-all-start.3
  27.1 0.0 copy-done.4
  27.1 11.6 %multiply_convert_fusion = (bf16[8,256,1408]{2,1,0:T(8,128)(2,1)}, bf16[8,256,1408]{2,1,0:T(8,128)(2,1)}) fusion(bf16[8,256,1408]{2,1,0:T(8,128)(2,1)} %param.10, f32[256]{0:T(256)S(1)} %copy-done.4, bf16[8,256,1408]{2,1,0:T(8,128)(2,1)} %param.9), kind=kLoop, calls=%fused_computation.7 | loop fusion | flops 17301504 | bytes 23069696 | tf_op jit(solution)/shard_map/convert_element_type | solution.py:30
  38.8 22.8 %all-to-all-done.3 = bf16[8,192,512]{2,1,0:T(8,128)(2,1)S(1)} async-done(((bf16[8,192,512]{2,1,0:T(8,128)(2,1)}), bf16[8,192,512]{2,1,0:T(8,128)(2,1)S(1)}, u32[]{:S(2)}, u32[]{:S(2)}) %all-to-all-start.3) | async-done | bytes 1572896 | tf_op jit(solution)/shard_map/all_to_all | solution.py:45
  61.6 0.0 copy-start.1
  61.6 130.4 %all_to_all.60 = bf16[8,256,1408]{2,1,0:T(8,128)(2,1)} all-to-all(bf16[8,256,1408]{2,1,0:T(8,128)(2,1)} %get-tuple-element.7), channel_id=1, replica_groups=mesh['fs'=8,'tp'=4] {'fs'}, dimensions={0} | all-to-all | bytes 11534336 | tf_op jit(solution)/shard_map/all_to_all | solution.py:36
  192.0 0.0 copy-done.1
  192.0 7.2 %all-to-all-start.1 = ((bf16[8,256,1408]{2,1,0:T(8,128)(2,1)}), bf16[8,256,1408]{2,1,0:T(8,128)(2,1)}, u32[]{:S(2)}, u32[]{:S(2)}) async-start(bf16[8,256,1408]{2,1,0:T(8,128)(2,1)} %get-tuple-element.6), calls=%async_computation.1 | async-start | bytes 11534336 | tf_op jit(solution)/shard_map/all_to_all | solution.py:37
  199.2 0.0 all-gather.2.cloned.1.call-start
  199.2 0.7 all-gather.2.cloned.1.call-update
  199.9 123.6 %all-to-all-done.1 = bf16[8,256,1408]{2,1,0:T(8,128)(2,1)} async-done(((bf16[8,256,1408]{2,1,0:T(8,128)(2,1)}), bf16[8,256,1408]{2,1,0:T(8,128)(2,1)}, u32[]{:S(2)}, u32[]{:S(2)}) %all-to-all-start.1) | async-done | bytes 5767200 | tf_op jit(solution)/shard_map/all_to_all | solution.py:37
  323.5 6.5 %all-to-all-start.2 = ((bf16[8,256,1408]{2,1,0:T(8,128)(2,1)}), bf16[8,256,1408]{2,1,0:T(8,128)(2,1)}, u32[]{:S(2)}, u32[]{:S(2)}) async-start(bf16[8,256,1408]{2,1,0:T(8,128)(2,1)} %param.11), calls=%async_computation.2 | async-start | bytes 11534336 | tf_op jit(solution)/shard_map/all_to_all | solution.py:38
  330.0 0.0 reduce-scatter.2.cloned.1.call-start
  330.0 0.0 all-gather.2.cloned.1.call-done
  330.0 0.0 copy-start
  330.0 4.2 fusion
  334.2 0.3 copy-done
  334.6 13.8 %fusion.9 = f32[1536,1408]{1,0:T(8,128)} fusion(bf16[2048,1408]{1,0:T(8,128)(2,1)} %bitcast.49, bf16[1536,2048]{1,0:T(8,128)(2,1)S(1)} %copy-done, f32[1536]{0:T(1024)S(1)} %add_rsqrt_fusion), kind=kOutput, calls=%fused_computation.15 | convolution fusion | flops 8867807232 | bytes 20715520 | tf_op jit(solution)/shard_map/dot_general | solution.py:50
  348.3 105.9 %all-to-all-done.2 = bf16[8,256,1408]{2,1,0:T(8,128)(2,1)} async-done(((bf16[8,256,1408]{2,1,0:T(8,128)(2,1)}), bf16[8,256,1408]{2,1,0:T(8,128)(2,1)}, u32[]{:S(2)}, u32[]{:S(2)}) %all-to-all-start.2) | async-done | bytes 5767200 | tf_op jit(solution)/shard_map/all_to_all | solution.py:38
  454.2 28.8 %fusion.5 = bf16[2048,1536]{0,1:T(8,128)(2,1)} fusion(bf16[2048,1408]{1,0:T(8,128)(2,1)} %bitcast.10, bf16[2048,1408]{1,0:T(8,128)(2,1)} %bitcast.9, f32[1536,1408]{1,0:T(8,128)} %fusion.9, bf16[1536,2048]{1,0:T(8,128)(2,1)} %all-gather.2.cloned.1.call-done, f32[1536]{0:T(1024)S(1)} %add_rsqrt_fusion), kind=kOutput, calls=%fused_computation.13 | convolution fusion | flops 17742299136 | bytes 32774144 | tf_op jit(solution)/shard_map/dot_general | solution.py:55
  483.1 0.0 copy-start.3
  483.1 0.0 copy-start.2
  483.1 0.0 reduce-scatter.2.cloned.1.call-update
  483.1 58.7 %reduce-scatter.2.cloned.1.call-done = bf16[512,1536]{0,1:T(8,128)(2,1)} async-done(((bf16[2048,1536]{0,1:T(8,128)(2,1)}), bf16[512,1536]{0,1:T(8,128)(2,1)}) %reduce-scatter.2.cloned.1.call-update) | async-done | bytes 1572880 | tf_op jit(solution)/shard_map/reduce_scatter | solution.py:54
  541.8 5.5 all-to-all-start.4
  547.3 0.2 reduce_sum.23
  547.5 0.1 copy.25
  547.6 0.0 copy-done.3
  547.6 0.0 copy-done.2
  547.7 34.1 %all-to-all-done.4 = bf16[512,8,192]{0,2,1:T(8,128)(2,1)S(1)} async-done(((bf16[512,8,192]{0,2,1:T(8,128)(2,1)}), bf16[512,8,192]{0,2,1:T(8,128)(2,1)S(1)}, u32[]{:S(2)}, u32[]{:S(2)}) %all-to-all-start.4) | async-done | bytes 1572896 | tf_op jit(solution)/shard_map/all_to_all | solution.py:62
  581.8 2.7 gather_fusion.1
  584.5 0.3 gather.11
  584.8 0.2 fusion.15
  585.0 0.9 fusion.16
  585.9 5.6 copy.34
  591.5 5.6 copy.35
  597.1 5.6 copy.36
  (9 shorter events, 0.1 us)
Async XLA Ops:
  16.0 11.1 %copy-start.4 = (f32[256]{0:T(256)S(1)}, f32[256]{0:T(256)}, u32[]{:S(2)}) copy-start(f32[256]{0:T(256)} %param.8) | copy-start | bytes 3076
  21.4 40.1 %all-to-all-start.3 = ((bf16[8,192,512]{2,1,0:T(8,128)(2,1)}), bf16[8,192,512]{2,1,0:T(8,128)(2,1)S(1)}, u32[]{:S(2)}, u32[]{:S(2)}) async-start(bf16[8,192,512]{2,1,0:T(8,128)(2,1)} %bitcast.6), calls=%async_computation.3 | async-start | bytes 3145728 | tf_op jit(solution)/shard_map/all_to_all | solution.py:45
  61.6 130.4 %copy-start.1 = (bf16[8,192,512]{2,1,0:T(8,128)(2,1)}, bf16[8,192,512]{2,1,0:T(8,128)(2,1)S(1)}, u32[]{:S(2)}) copy-start(bf16[8,192,512]{2,1,0:T(8,128)(2,1)S(1)} %all-to-all-done.3) | copy-start | bytes 4718596
  192.0 131.5 %all-to-all-start.1 = ((bf16[8,256,1408]{2,1,0:T(8,128)(2,1)}), bf16[8,256,1408]{2,1,0:T(8,128)(2,1)}, u32[]{:S(2)}, u32[]{:S(2)}) async-start(bf16[8,256,1408]{2,1,0:T(8,128)(2,1)} %get-tuple-element.6), calls=%async_computation.1 | async-start | bytes 11534336 | tf_op jit(solution)/shard_map/all_to_all | solution.py:37
  199.2 130.8 %all-gather.2.cloned.1.call-start = ((), (), s32[]{:S(2)}) async-start(), calls=%async_computation.6 | async-start | bytes 7864320 | tf_op jit(solution)/shard_map/all_gather | solution.py:46
  323.5 130.7 %all-to-all-start.2 = ((bf16[8,256,1408]{2,1,0:T(8,128)(2,1)}), bf16[8,256,1408]{2,1,0:T(8,128)(2,1)}, u32[]{:S(2)}, u32[]{:S(2)}) async-start(bf16[8,256,1408]{2,1,0:T(8,128)(2,1)} %param.11), calls=%async_computation.2 | async-start | bytes 11534336 | tf_op jit(solution)/shard_map/all_to_all | solution.py:38
  330.0 211.9 %reduce-scatter.2.cloned.1.call-start = ((), (), s32[]{:S(2)}) async-start(), calls=%async_computation.7 | async-start | bytes 7864320 | tf_op jit(solution)/shard_map/reduce_scatter | solution.py:54
  330.0 4.6 copy-start
  483.1 64.5 %copy-start.3 = (f32[384,2]{0,1:T(2,128)S(1)}, f32[384,2]{0,1:T(2,128)}, u32[]{:S(2)}) copy-start(f32[384,2]{0,1:T(2,128)} %param.13) | copy-start | bytes 9220
  483.1 64.6 %copy-start.2 = (s32[384,2]{0,1:T(2,128)S(1)}, s32[384,2]{0,1:T(2,128)}, u32[]{:S(2)}) copy-start(s32[384,2]{0,1:T(2,128)} %param.12) | copy-start | bytes 9220
  541.8 40.0 %all-to-all-start.4 = ((bf16[512,8,192]{0,2,1:T(8,128)(2,1)}), bf16[512,8,192]{0,2,1:T(8,128)(2,1)S(1)}, u32[]{:S(2)}, u32[]{:S(2)}) async-start(bf16[512,8,192]{0,2,1:T(8,128)(2,1)} %bitcast.53), calls=%async_computation.5 | async-start | bytes 3145728 | tf_op jit(solution)/shard_map/all_to_all | solution.py:62
Sparse Core Ops, SparseCore 0:
  202.1 48.2 all-gather.1
  483.2 58.5 reduce-scatter.1
where the time goes:
time: 615 us; the launch traced here: 610 us
  waiting for transfers between devices  346 us (56%)
  blocking collectives  130 us (21%)
  matrix products  42.6 us (7%)
  local copies, waits for them, and re-layouts  31.9 us (5%)
  starting transfers between devices  24.8 us (4%)
  other arithmetic  19.7 us (3%)
  between operations  14.2 us (2%)
    all_to_all x1, blocking collectives, shards(): lax.all_to_all(spread(gate_low), 'fs', split_axis=0, concat_axis=1, tiled...  130 us
    all_to_all x1, waiting for transfers between devices, shards(): lax.all_to_all(spread(up_low), 'fs', split_axis=0, concat_axis=1, tiled=T...  124 us
    all_to_all x1, waiting for transfers between devices, shards(): lax.all_to_all(spread(down_train), 'fs', split_axis=0, concat_axis=1, til...  106 us
    reduce_scatter x1, waiting for transfers between devices, shards(): lax.psum_scatter(lax.dot_general(down_matrix, active, (((1,), (1,)), ((),...  58.7 us
    all_to_all x1, waiting for transfers between devices, shards(): lax.all_to_all(summed, 'fs', split_axis=1, concat_axis=1, tiled=True)  34.1 us
    dot_general x1, matrix products, shards(): lax.dot_general(down_matrix, active, (((1,), (1,)), ((), ())), preferred_...  28.8 us
    all_to_all x1, waiting for transfers between devices, shards(): lax.all_to_all(outgoing, 'fs', split_axis=0, concat_axis=0, tiled=True)  22.8 us
    unnamed x14, local copies, waits for them, and re-layouts  18 us
  transfers between devices with their start and end apart: 6, of which 5 were waited for; matrix products, arithmetic and copies ran while one was open for 5% of the time, Pallas kernels for 0%

commit v1 on v0

v1 whole, which is shorter than its diff:
```python
import functools

import jax
import jax.numpy as jnp
from jax import lax
from jax.experimental import pallas as pl
from jax.experimental.pallas import tpu as pltpu
from jax.sharding import PartitionSpec as P

EXPERTS = 8
EPSILON = 1e-06
MESH = pl.DeviceIdType.MESH
F32 = jnp.float32
BF16 = jnp.bfloat16
NT = (((1,), (1,)), ((), ()))
TN = (((0,), (0,)), ((), ()))


def shift_of(step, n):
    return n // 2 + (1 - 2 * (step % 2)) * ((step + 1) // 2)


def kernel(
    n, m, tokens, gain, gate_hbm, up_hbm, down_hbm, routes, logits,
    gate_out, up_out, down_out, mixed,
    stage, weights, outgoing, rows, active, picks, ranks, scales, mix_high, mix_low,
    parts, landed, result, returned,
    load_sem, w_send, w_recv, d_send, d_recv, f_send, f_recv, p_send, p_recv, r_send, r_recv, o_sem,
):
    me = lax.axis_index("fs")
    tp = lax.axis_index("tp")
    copies = n // EXPERTS
    tok_rows, feats = tokens.shape
    cap = tok_rows // 2 // copies
    slots = n * cap
    depth = weights.shape[1] // n
    per = n // m

    def load(w, e):
        source = (gate_hbm, up_hbm)[w]
        return pltpu.make_async_copy(source.at[e], stage.at[w, e], load_sem.at[w, e])

    for w in range(2):
        for e in range(EXPERTS):
            load(w, e).start()
    mine = weights.at[2, pl.ds(pl.multiple_of(me * depth, depth), depth)]
    own_down = pltpu.make_async_copy(down_hbm.at[me % EXPERTS], mine, load_sem.at[2, 0])
    own_down.start()

    barrier = pltpu.get_barrier_semaphore()

    @pl.loop(1, n)
    def _(k):
        pl.semaphore_signal(
            barrier, inc=1, device_id=((me + k) % n, tp), device_id_type=MESH
        )

    @pl.loop(1, m)
    def _(k):
        pl.semaphore_signal(
            barrier, inc=1, device_id=(me, (tp + k) % m), device_id_type=MESH
        )

    first, second = routes[0:1, :], routes[1:2, :]
    ids = lax.broadcasted_iota(jnp.int32, (EXPERTS, tok_rows), 0)
    named = ((ids == first) | (ids == second)).astype(F32)
    before = lax.broadcasted_iota(jnp.int32, (tok_rows, tok_rows), 0)
    after = lax.broadcasted_iota(jnp.int32, (tok_rows, tok_rows), 1)
    earlier = (before < after).astype(F32).astype(BF16)
    picks[...] = named
    ranks[...] = jnp.dot(named.astype(BF16), earlier, preferred_element_type=F32)
    gap = logits[0:1, :] - logits[1:2, :]
    scales[...] = jnp.where(ids == first, jax.nn.sigmoid(gap), jax.nn.sigmoid(-gap))

    pl.semaphore_wait(barrier, n - 1 + m - 1)

    def dispatch(k):
        target = (me + k) % n
        return pltpu.make_async_remote_copy(
            src_ref=outgoing.at[pl.ds(pl.multiple_of(target * cap, cap), cap)],
            dst_ref=rows.at[
                pl.ds(pl.multiple_of(me * cap, cap), cap),
                pl.ds(pl.multiple_of(tp * feats, feats), feats),
            ],
            send_sem=d_send.at[k],
            recv_sem=d_recv.at[k],
            device_id=(target, tp),
            device_id_type=MESH,
        )

    def fill(target):
        e = target % EXPERTS
        want = (
            lax.broadcasted_iota(jnp.int32, (cap, tok_rows), 0) * copies + target // EXPERTS
        ).astype(F32)
        hit = (ranks[pl.ds(e, 1), :] == want) & (picks[pl.ds(e, 1), :] > 0.5)
        where = pl.ds(pl.multiple_of(target * cap, cap), cap)
        chosen = jnp.where(hit, 1.0, 0.0).astype(BF16)
        moved = jnp.dot(chosen, tokens[...], preferred_element_type=F32).astype(BF16)
        outgoing[where, :] = moved
        scale = jnp.where(hit, scales[pl.ds(e, 1), :], 0.0)
        high = scale.astype(BF16)
        mix_high[where, :] = high
        mix_low[where, :] = (scale - high.astype(F32)).astype(BF16)
        return moved

    @pl.loop(0, n - 1)
    def _(i):
        k = shift_of(i, n)
        fill((me + k) % n)
        dispatch(k).start()

    rows[
        pl.ds(pl.multiple_of(me * cap, cap), cap),
        pl.ds(pl.multiple_of(tp * feats, feats), feats),
    ] = fill(me)

    def give(w, k):
        target = (me + k) % n
        e = target % EXPERTS
        return pltpu.make_async_remote_copy(
            src_ref=down_hbm.at[e] if w == 2 else stage.at[w, e],
            dst_ref=weights.at[w, pl.ds(pl.multiple_of(me * depth, depth), depth)],
            send_sem=w_send.at[w, k],
            recv_sem=w_recv.at[w, k],
            device_id=(target, tp),
            device_id_type=MESH,
        )

    for w in range(2):
        for e in range(EXPERTS):
            load(w, e).wait()

        @pl.loop(0, EXPERTS)
        def _(e):
            stage[w, pl.ds(e, 1)] = (
                stage[w, pl.ds(e, 1)].astype(F32) * gain[...][None]
            ).astype(BF16)

        @pl.loop(0, n - 1)
        def _(i):
            give(w, shift_of(i, n)).start()

        weights[w, pl.ds(pl.multiple_of(me * depth, depth), depth), :] = stage[
            w, pl.ds(me % EXPERTS, 1)
        ][0]

    @pl.loop(0, n - 1)
    def _(i):
        give(2, shift_of(i, n)).start()

    def share(k):
        block = rows.at[:, pl.ds(pl.multiple_of(tp * feats, feats), feats)]
        return pltpu.make_async_remote_copy(
            src_ref=block,
            dst_ref=block,
            send_sem=f_send.at[k],
            recv_sem=f_recv.at[k],
            device_id=(me, (tp + k) % m),
            device_id_type=MESH,
        )

    @pl.loop(1, n)
    def _(k):
        dispatch(k).wait()

    @pl.loop(1, m)
    def _(k):
        share(k).start()

    @pl.loop(1, m)
    def _(k):
        share(k).wait()

    tile = slots // 12

    @pl.loop(0, slots // tile)
    def _(i):
        where = pl.ds(pl.multiple_of(i * tile, tile), tile)
        value = rows[where, :].astype(F32)
        inverse = lax.rsqrt(jnp.mean(value * value, axis=1, keepdims=True) + EPSILON)
        rows[where, :] = (value * inverse).astype(BF16)

    outs = []
    for w in range(2):

        @pl.loop(1, n)
        def _(k):
            give(w, k).wait()

        outs.append(
            pltpu.make_async_copy(weights.at[w], (gate_out, up_out)[w].at[0], o_sem.at[w])
        )
        outs[w].start()

    big = slots // 6

    @pl.loop(0, slots // big)
    def _(i):
        where = pl.ds(pl.multiple_of(i * big, big), big)
        value = rows[where, :]
        gate_val = jnp.dot(value, weights[0], preferred_element_type=F32)
        up_val = jnp.dot(value, weights[1], preferred_element_type=F32)
        active[where, :] = (gate_val / (1.0 + jnp.exp(-gate_val)) * up_val).astype(BF16)

    def source_of(i):
        k = jnp.where(i == 0, 0, shift_of(jnp.maximum(i - 1, 0), n))
        return k, (me + n - k) % n

    def hand(j):
        owner = j // per
        k = (owner + m - tp) % m
        return pltpu.make_async_remote_copy(
            src_ref=parts.at[j],
            dst_ref=landed.at[j % per, k],
            send_sem=p_send.at[j],
            recv_sem=p_recv.at[j % per, k],
            device_id=(me, owner),
            device_id_type=MESH,
        )

    def taken(q, k):
        return pltpu.make_async_remote_copy(
            src_ref=parts.at[0],
            dst_ref=landed.at[q, k],
            send_sem=p_send.at[0],
            recv_sem=p_recv.at[q, k],
            device_id=(me, (tp + k) % m),
            device_id_type=MESH,
        )

    def back(q, k):
        target = (me + k) % n
        return pltpu.make_async_remote_copy(
            src_ref=result.at[q, pl.ds(pl.multiple_of(target * cap, cap), cap)],
            dst_ref=returned.at[q, pl.ds(pl.multiple_of(me * cap, cap), cap)],
            send_sem=r_send.at[q, k],
            recv_sem=r_recv.at[q, k],
            device_id=(target, tp),
            device_id_type=MESH,
        )

    own_down.wait()
    half = slots // 4

    @pl.loop(0, n + 1)
    def _(i):
        @pl.when(i < n)
        def _():
            k, j = source_of(i)

            @pl.when(i > 0)
            def _():
                give(2, k).wait()

            rhs = weights[2, pl.ds(pl.multiple_of(j * depth, depth), depth), :]

            @pl.loop(0, slots // half)
            def _(r):
                where = pl.ds(pl.multiple_of(r * half, half), half)
                parts[j, where, :] = lax.dot_general(
                    active[where, :], rhs, NT, preferred_element_type=F32
                ).astype(BF16)

            @pl.when(j // per != tp)
            def _():
                hand(j).start()

        @pl.when(i > 0)
        def _():
            _, j = source_of(jnp.maximum(i - 1, 0))
            q = j % per

            @pl.when(j // per == tp)
            def _():
                @pl.loop(1, m)
                def _(k):
                    taken(q, k).wait_recv()

                @pl.loop(0, slots // half)
                def _(r):
                    where = pl.ds(pl.multiple_of(r * half, half), half)
                    total = parts[j, where, :].astype(F32)
                    for k in range(1, m):
                        total = total + landed[q, k, where, :].astype(F32)
                    result[q, where, :] = total.astype(BF16)

                @pl.loop(0, n - 1)
                def _(s):
                    back(q, shift_of(s, n)).start()

                mine = pl.ds(pl.multiple_of(me * cap, cap), cap)
                returned[q, mine, :] = result[q, mine, :]

    last = pltpu.make_async_copy(weights.at[2], down_out.at[0], o_sem.at[2])
    last.start()

    @pl.loop(0, n)
    def _(j):
        @pl.when(j // per != tp)
        def _():
            hand(j).wait_send()

    for q in range(per):

        @pl.loop(1, n)
        def _(k):
            back(q, k).wait()

        value = returned[q]
        total = lax.dot_general(mix_high[...], value, TN, preferred_element_type=F32)
        total += lax.dot_general(mix_low[...], value, TN, preferred_element_type=F32)
        mixed[:, q * depth : (q + 1) * depth] = total.astype(BF16)

    for out in outs:
        out.wait()
    last.wait()


def shards(n, m, tokens, norm_gain, gate_train, up_train, down_train, routes, route_logits):
    experts, depth, width = gate_train.shape
    tok_rows, feats = tokens.shape
    copies = n // experts
    cap = tok_rows // 2 // copies
    slots = n * cap
    per = n // m
    full = jax.ShapeDtypeStruct((1, depth * n, width), BF16)
    vmem = pl.BlockSpec(memory_space=pltpu.VMEM)
    hbm = pl.BlockSpec(memory_space=pl.ANY)
    dma = pltpu.SemaphoreType.DMA
    return pl.pallas_call(
        functools.partial(kernel, n, m),
        out_shape=(full, full, full, jax.ShapeDtypeStruct((tok_rows, feats), BF16)),
        in_specs=[vmem, vmem, hbm, hbm, hbm, vmem, vmem],
        out_specs=(hbm, hbm, hbm, vmem),
        scratch_shapes=[
            pltpu.VMEM((2, experts, depth, width), BF16),
            pltpu.VMEM((3, depth * n, width), BF16),
            pltpu.VMEM((slots, feats), BF16),
            pltpu.VMEM((slots, feats * m), BF16),
            pltpu.VMEM((slots, width), BF16),
            pltpu.VMEM((experts, tok_rows), F32),
            pltpu.VMEM((experts, tok_rows), F32),
            pltpu.VMEM((experts, tok_rows), F32),
            pltpu.VMEM((slots, tok_rows), BF16),
            pltpu.VMEM((slots, tok_rows), BF16),
            pltpu.VMEM((n, slots, depth), BF16),
            pltpu.VMEM((per, m, slots, depth), BF16),
            pltpu.VMEM((per, slots, depth), BF16),
            pltpu.VMEM((per, slots, depth), BF16),
            dma((3, experts)),
            dma((3, n)),
            dma((3, n)),
            dma((n,)),
            dma((n,)),
            dma((m,)),
            dma((m,)),
            dma((n,)),
            dma((per, m)),
            dma((per, n)),
            dma((per, n)),
            dma((3,)),
        ],
        compiler_params=pltpu.CompilerParams(
            collective_id=0, has_side_effects=True, vmem_limit_bytes=67043328
        ),
    )(
        tokens,
        norm_gain[:, None],
        gate_train,
        up_train,
        down_train,
        routes.T,
        route_logits.T,
    )


def solution(mesh):
    weight = P(None, "fs", "tp")
    placed = (P("fs", "tp"), P("fs"), weight, weight, weight, P("fs", None), P("fs", None))
    copy = P("fs", None, "tp")
    return jax.shard_map(
        functools.partial(shards, mesh.shape["fs"], mesh.shape["tp"]),
        mesh=mesh,
        in_specs=placed,
        out_specs=(copy, copy, copy, P("fs", "tp")),
        check_vma=False,
    )
```

time: 615 us -> 501 us (0.81)
  Pallas kernels: 0 us -> 485 us
  waiting for transfers between devices: 346 us -> 0 us
  blocking collectives: 130 us -> 0 us
  matrix products: 42.6 us -> 0 us
  starting transfers between devices: 24.8 us -> 0 us
  other arithmetic: 19.7 us -> 0 us
  local copies, waits for them, and re-layouts: 31.9 us -> 15.2 us
  between operations: 14.2 us -> 0.65 us
    pallas_call x0 -> x1, Pallas kernels: none -> 485 us  [shards(): pl.pallas_call(functools.partial(kernel, n, m), out_shape=(full, full, fu...]
    all_to_all x4 -> x0, waiting for transfers between devices: 286 us -> none  [the longest x1 124 us: shards(): lax.all_to_all(spread(up_low), 'fs', split_axis=0, concat_axis=1, tiled=T...]
    all_to_all x1 -> x0, blocking collectives: 130 us -> none  [shards(): lax.all_to_all(spread(gate_low), 'fs', split_axis=0, concat_axis=1, tiled...]
    reduce_scatter x1 -> x0, waiting for transfers between devices: 58.7 us -> none  [shards(): lax.psum_scatter(lax.dot_general(down_matrix, active, (((1,), (1,)), ((),...]
    dot_general x2 -> x0, matrix products: 42.6 us -> none  [the longest x1 28.8 us: shards(): lax.dot_general(down_matrix, active, (((1,), (1,)), ((), ())), preferred_...]
    all_to_all x4 -> x0, starting transfers between devices: 24.8 us -> none  [the longest x1 7.19 us: shards(): lax.all_to_all(spread(up_low), 'fs', split_axis=0, concat_axis=1, tiled=T...]
    convert_element_type x4 -> x0, other arithmetic: 12.8 us -> none  [the longest x1 11.6 us: shards(): up_low = (up_train.astype(jnp.float32) * gain_rows).astype(jnp.bfloat16)]
    gather x3 -> x0, local copies, waits for them, and re-layouts: 8.38 us -> none  [the longest x1 5.41 us: shards(): outgoing = padded[owner]]
  transfers between devices with their start and end apart: 6 -> 0, of which waited for: 5 -> 0; matrix products, arithmetic and copies ran while one was open for 5% -> 0% of each run, Pallas kernels for 0% -> 0%
where the time goes in v1:
time: 501 us
  Pallas kernels  485 us (97%)
  local copies, waits for them, and re-layouts  15.2 us (3%)
    pallas_call x1, Pallas kernels, shards(): pl.pallas_call(functools.partial(kernel, n, m), out_shape=(full, full, fu...  485 us
    unnamed x10, local copies, waits for them, and re-layouts  13.7 us

profile of v1, /device:TPU:15, one launch (start us, length us, event | category | flops | bytes accessed | tf_op | source)
XLA Modules:
  0.0 500.7 jit_solution(8327093127999699926)
XLA Ops:
  0.6 1.5 copy.11.gain
  2.1 484.8 %shard_map.102 = (bf16[1,2048,1408]{2,1,0:T(8,128)(2,1)}, bf16[1,2048,1408]{2,1,0:T(8,128)(2,1)}, bf16[1,2048,1408]{2,1,0:T(8,128)(2,1)}, bf16[384,512]{1,0:T(8,128)(2,1)}) custom-call(bf16[384,512]{1,0:T(8,128)(2,1)} %tokens.1, f32[256,1]{1,0:T(8,128)} %copy.11.gain, bf16[8,256,1408]{2,1,0:T(8,128)(2,1)} %gate_hbm.1, bf16[8,256,1408]{2,1,0:T(8,128)(2,1)} %up_hbm.1, ...), custom_call_target="tpu_custom_call" | custom-call | tf_op jit(solution)/shard_map/pallas_call | solution.py:331
  486.9 0.0 copy-start.1
  486.9 5.7 %copy.16 = bf16[1,2048,1408]{2,1,0:T(8,128)(2,1)} copy(bf16[1,2048,1408]{2,1,0:T(8,128)(2,1)} %get-tuple-element.8) | data formatting | bytes 11534336
  492.7 0.0 copy-done.1
  492.7 0.0 copy-start
  492.7 2.9 copy.17
  495.6 1.8 copy-done
  497.4 0.0 copy-start.2
  497.4 2.5 copy.18
  499.9 0.0 copy-done.2
  499.9 0.7 copy.19
Async XLA Ops:
  486.9 5.8 %copy-start.1 = (bf16[1,2048,1408]{2,1,0:T(8,128)(2,1)S(1)}, bf16[1,2048,1408]{2,1,0:T(8,128)(2,1)}, u32[]{:S(2)}) copy-start(bf16[1,2048,1408]{2,1,0:T(8,128)(2,1)} %get-tuple-element.9) | copy-start | bytes 17301508
  492.7 4.7 copy-start
  497.4 2.5 copy-start.2

commit v2 on v1

--- a/solution.py
+++ b/solution.py
@@ -23,9 +23,9 @@
 def kernel(
     n, m, tokens, gain, gate_hbm, up_hbm, down_hbm, routes, logits,
     gate_out, up_out, down_out, mixed,
-    stage, weights, outgoing, rows, active, picks, ranks, scales, mix_high, mix_low,
+    stage, weights, gathered, tables, rows, active, ranks, scales, mix_high, mix_low,
     parts, landed, result, returned,
-    load_sem, w_send, w_recv, d_send, d_recv, f_send, f_recv, p_send, p_recv, r_send, r_recv, o_sem,
+    load_sem, w_send, w_recv, a_send, a_recv, b_send, b_recv, f_send, f_recv, p_send, p_recv, r_send, r_recv, o_sem,
 ):
     me = lax.axis_index("fs")
     tp = lax.axis_index("tp")
@@ -67,53 +67,64 @@
     before = lax.broadcasted_iota(jnp.int32, (tok_rows, tok_rows), 0)
     after = lax.broadcasted_iota(jnp.int32, (tok_rows, tok_rows), 1)
     earlier = (before < after).astype(F32).astype(BF16)
-    picks[...] = named
-    ranks[...] = jnp.dot(named.astype(BF16), earlier, preferred_element_type=F32)
+    rank = jnp.dot(named.astype(BF16), earlier, preferred_element_type=F32)
+    ranks[...] = jnp.where(named > 0.5, rank, -1.0)
     gap = logits[0:1, :] - logits[1:2, :]
     scales[...] = jnp.where(ids == first, jax.nn.sigmoid(gap), jax.nn.sigmoid(-gap))
 
     pl.semaphore_wait(barrier, n - 1 + m - 1)
 
-    def dispatch(k):
-        target = (me + k) % n
-        return pltpu.make_async_remote_copy(
-            src_ref=outgoing.at[pl.ds(pl.multiple_of(target * cap, cap), cap)],
-            dst_ref=rows.at[
-                pl.ds(pl.multiple_of(me * cap, cap), cap),
-                pl.ds(pl.multiple_of(tp * feats, feats), feats),
-            ],
-            send_sem=d_send.at[k],
-            recv_sem=d_recv.at[k],
+    side = n // 2
+    base = me // side * side
+    partner = (me + side) % n
+
+    def spread(w, k):
+        target = jnp.where(k == 0, partner, base + (me + k) % side)
+        return pltpu.make_async_remote_copy(
+            src_ref=(tokens, ranks)[w],
+            dst_ref=(gathered, tables)[w].at[me],
+            send_sem=a_send.at[w, k],
+            recv_sem=a_recv.at[w, k],
             device_id=(target, tp),
             device_id_type=MESH,
         )
 
-    def fill(target):
+    def relay(w, k):
+        block = (gathered, tables)[w].at[partner]
+        return pltpu.make_async_remote_copy(
+            src_ref=block,
+            dst_ref=block,
+            send_sem=b_send.at[w, k],
+            recv_sem=b_recv.at[w, k],
+            device_id=(base + (me + k) % side, tp),
+            device_id_type=MESH,
+        )
+
+    @pl.loop(0, side)
+    def _(k):
+        for w in range(2):
+            spread(w, k).start()
+
+    def mix(target):
         e = target % EXPERTS
         want = (
             lax.broadcasted_iota(jnp.int32, (cap, tok_rows), 0) * copies + target // EXPERTS
         ).astype(F32)
-        hit = (ranks[pl.ds(e, 1), :] == want) & (picks[pl.ds(e, 1), :] > 0.5)
+        scale = jnp.where(ranks[pl.ds(e, 1), :] == want, scales[pl.ds(e, 1), :], 0.0)
         where = pl.ds(pl.multiple_of(target * cap, cap), cap)
-        chosen = jnp.where(hit, 1.0, 0.0).astype(BF16)
-        moved = jnp.dot(chosen, tokens[...], preferred_element_type=F32).astype(BF16)
-        outgoing[where, :] = moved
-        scale = jnp.where(hit, scales[pl.ds(e, 1), :], 0.0)
         high = scale.astype(BF16)
         mix_high[where, :] = high
         mix_low[where, :] = (scale - high.astype(F32)).astype(BF16)
-        return moved
-
-    @pl.loop(0, n - 1)
-    def _(i):
-        k = shift_of(i, n)
-        fill((me + k) % n)
-        dispatch(k).start()
-
-    rows[
-        pl.ds(pl.multiple_of(me * cap, cap), cap),
-        pl.ds(pl.multiple_of(tp * feats, feats), feats),
-    ] = fill(me)
+
+    def fill(source, tok, table):
+        want = (
+            lax.broadcasted_iota(jnp.int32, (cap, tok_rows), 0) * copies + me // EXPERTS
+        ).astype(F32)
+        chosen = jnp.where(table == want, 1.0, 0.0).astype(BF16)
+        rows[
+            pl.ds(pl.multiple_of(source * cap, cap), cap),
+            pl.ds(pl.multiple_of(tp * feats, feats), feats),
+        ] = jnp.dot(chosen, tok, preferred_element_type=F32).astype(BF16)
 
     def give(w, k):
         target = (me + k) % n
@@ -137,7 +148,22 @@
                 stage[w, pl.ds(e, 1)].astype(F32) * gain[...][None]
             ).astype(BF16)
 
-        @pl.loop(0, n - 1)
+        ahead = 1 if w == 0 else 0
+
+        @pl.loop(0, ahead)
+        def _(i):
+            give(w, shift_of(i, n)).start()
+
+        if w == 0:
+            for v in range(2):
+                spread(v, 0).wait()
+
+            @pl.loop(1, side)
+            def _(k):
+                for v in range(2):
+                    relay(v, k).start()
+
+        @pl.loop(ahead, n - 1)
         def _(i):
             give(w, shift_of(i, n)).start()
 
@@ -147,7 +173,7 @@
 
     @pl.loop(0, n - 1)
     def _(i):
-        give(2, shift_of(i, n)).start()
+        give(2, shift_of(n - 2 - i, n)).start()
 
     def share(k):
         block = rows.at[:, pl.ds(pl.multiple_of(tp * feats, feats), feats)]
@@ -160,13 +186,28 @@
             device_id_type=MESH,
         )
 
+    @pl.loop(1, side)
+    def _(k):
+        for w in range(2):
+            spread(w, k).wait()
+            relay(w, k).wait()
+
+    expert = pl.ds(me % EXPERTS, 1)
+
     @pl.loop(1, n)
     def _(k):
-        dispatch(k).wait()
+        source = (me + k) % n
+        fill(source, gathered[source], tables[source, expert, :])
+
+    fill(me, tokens[...], ranks[expert, :])
 
     @pl.loop(1, m)
     def _(k):
         share(k).start()
+
+    @pl.loop(0, n)
+    def _(d):
+        mix(d)
 
     @pl.loop(1, m)
     def _(k):
@@ -204,7 +245,7 @@
         active[where, :] = (gate_val / (1.0 + jnp.exp(-gate_val)) * up_val).astype(BF16)
 
     def source_of(i):
-        k = jnp.where(i == 0, 0, shift_of(jnp.maximum(i - 1, 0), n))
+        k = jnp.where(i == 0, 0, shift_of(n - 2 - jnp.maximum(i - 1, 0), n))
         return k, (me + n - k) % n
 
     def hand(j):
@@ -336,10 +377,10 @@
         scratch_shapes=[
             pltpu.VMEM((2, experts, depth, width), BF16),
             pltpu.VMEM((3, depth * n, width), BF16),
-            pltpu.VMEM((slots, feats), BF16),
+            pltpu.VMEM((n, tok_rows, feats), BF16),
+            pltpu.VMEM((n, experts, tok_rows), F32),
             pltpu.VMEM((slots, feats * m), BF16),
             pltpu.VMEM((slots, width), BF16),
-            pltpu.VMEM((experts, tok_rows), F32),
             pltpu.VMEM((experts, tok_rows), F32),
             pltpu.VMEM((experts, tok_rows), F32),
             pltpu.VMEM((slots, tok_rows), BF16),
@@ -351,8 +392,10 @@
             dma((3, experts)),
             dma((3, n)),
             dma((3, n)),
-            dma((n,)),
-            dma((n,)),
+            dma((2, n // 2)),
+            dma((2, n // 2)),
+            dma((2, n // 2)),
+            dma((2, n // 2)),
             dma((m,)),
             dma((m,)),
             dma((n,)),

time: 501 us -> 499 us (level)
  Pallas kernels: 485 us -> 479 us
    pallas_call x1, Pallas kernels: 485 us -> 479 us  [shards(): pl.pallas_call(functools.partial(kernel, n, m), out_shape=(full, full, fu...]
where the time goes in v2:
time: 499 us; the launch traced here: 495 us
  Pallas kernels  479 us (96%)
  local copies, waits for them, and re-layouts  15.2 us (3%)
    pallas_call x1, Pallas kernels, shards(): pl.pallas_call(functools.partial(kernel, n, m), out_shape=(full, full, fu...  479 us
    unnamed x10, local copies, waits for them, and re-layouts  13.7 us

profile of v2, /device:TPU:15, one launch (start us, length us, event | category | flops | bytes accessed | tf_op | source)
XLA Modules:
  0.0 495.2 jit_solution(6755945044929428589)
XLA Ops:
  0.6 1.5 copy.11.gain
  2.1 479.3 %shard_map.102 = (bf16[1,2048,1408]{2,1,0:T(8,128)(2,1)}, bf16[1,2048,1408]{2,1,0:T(8,128)(2,1)}, bf16[1,2048,1408]{2,1,0:T(8,128)(2,1)}, bf16[384,512]{1,0:T(8,128)(2,1)}) custom-call(bf16[384,512]{1,0:T(8,128)(2,1)} %tokens.1, f32[256,1]{1,0:T(8,128)} %copy.11.gain, bf16[8,256,1408]{2,1,0:T(8,128)(2,1)} %gate_hbm.1, bf16[8,256,1408]{2,1,0:T(8,128)(2,1)} %up_hbm.1, ...), custom_call_target="tpu_custom_call" | custom-call | tf_op jit(solution)/shard_map/pallas_call | solution.py:372
  481.4 0.0 copy-start.1
  481.4 5.7 %copy.16 = bf16[1,2048,1408]{2,1,0:T(8,128)(2,1)} copy(bf16[1,2048,1408]{2,1,0:T(8,128)(2,1)} %get-tuple-element.8) | data formatting | bytes 11534336
  487.2 0.0 copy-done.1
  487.2 0.0 copy-start
  487.2 2.9 copy.17
  490.1 1.8 copy-done
  491.9 0.0 copy-start.2
  491.9 2.5 copy.18
  494.4 0.0 copy-done.2
  494.4 0.7 copy.19
Async XLA Ops:
  481.4 5.8 %copy-start.1 = (bf16[1,2048,1408]{2,1,0:T(8,128)(2,1)S(1)}, bf16[1,2048,1408]{2,1,0:T(8,128)(2,1)}, u32[]{:S(2)}) copy-start(bf16[1,2048,1408]{2,1,0:T(8,128)(2,1)} %get-tuple-element.9) | copy-start | bytes 17301508
  487.2 4.7 copy-start
  491.9 2.5 copy-start.2
